TPU v7x, 32 devices: a whole 2x2x4 slice. The times are simulated.
32 devices in a mesh: ep: 8 (over z, y), tp: 4 (over x, core).
Axes of the slice: x: 2, y: 2, z: 4, core: 2. Of those that a mesh axis runs over, the one named last changes fastest.
Arguments:
- queries: bfloat16 [8192, 1024], P('ep', 'tp'), may hold values from -6 to 6
- key_rows: bfloat16 [8192, 256], P('ep', 'tp'), may hold values from -6 to 6
- values: bfloat16 [8192, 256], P('ep', 'tp'), may hold values from -6 to 6
- sink_logit: float32 [16], P('tp'), may hold values from 3 to 7
- out_weight: bfloat16 [1024, 2048], P('tp'), may hold values from -0.1875 to 0.1875
- out_gain: float32 [2048], replicated, may hold values from 0.1 to 1.9
- routed_tokens: bfloat16 [16384, 2048], P(('ep', 'tp')), may hold values from -6 to 6
- expert_ids: int32 [16384, 2], P(('ep', 'tp')), may hold values from 0 to 31, as said below
- route_weight: float32 [16384, 2], P(('ep', 'tp')), may hold values from 0.1 to 1
- routed_gain: float32 [2048], replicated, may hold values from 0.1 to 1.9
- expert_gate: bfloat16 [32, 2048, 1024], P('ep', None, 'tp'), may hold values from -0.125 to 0.125
- expert_up: bfloat16 [32, 2048, 1024], P('ep', None, 'tp'), may hold values from -0.125 to 0.125
- expert_down: bfloat16 [32, 2048, 1024], P('ep', None, 'tp'), may hold values from -0.1875 to 0.1875
Outputs:
- mixer_out: bfloat16 [8192, 2048], P(('ep', 'tp'))
- experts_out: bfloat16 [16384, 2048], P(('ep', 'tp'))
Inputs may be any that keep to these rules, and one draw needn't show every extreme that they name: `expert_ids`: both experts of a row lie in one group (equal id // 8); the 512 rows of one device name every group exactly 512 / 4 times; the rows of one device name no expert more than 64 times; in every device's rows some expert of each group is named exactly 64 times, and one expert is named exactly 64 times by the rows of every device.
All inputs are finite; a program needn't handle non-finite values.
Results may differ from a plain program's by a relative error of at most 0.0071.
Values may be sent and summed in bfloat16 or wider, within the bound.
A program may use at most 192 MiB of HBM per device.

v0:
```python
import jax
import jax.numpy as jnp
from jax import lax
from jax.sharding import PartitionSpec as P

HEAD_DIM = 64
WINDOW = 128
QBLOCK = 512
EXPERTS = 32
TOP = 2
CAP = 64
epsilon = 1e-06


def padded(block, sides, width):
    for axis, dim in sides:
        count = lax.axis_size(axis)
        forward = [(i, i + 1) for i in range(count - 1)]
        backward = [(target, source) for source, target in forward]
        low = lax.ppermute(
            lax.slice_in_dim(block, block.shape[dim] - width, None, axis=dim), axis, forward
        )
        high = lax.ppermute(lax.slice_in_dim(block, 0, width, axis=dim), axis, backward)
        block = jnp.concatenate([low, block, high], axis=dim)
    return block


def local(
    queries,
    key_rows,
    values,
    sink_logit,
    out_weight,
    out_gain,
    routed_tokens,
    expert_ids,
    route_weight,
    routed_gain,
    expert_gate,
    expert_up,
    expert_down,
):
    row_count = queries.shape[0]
    heads_here = queries.shape[1] // HEAD_DIM
    kv_here = key_rows.shape[1] // HEAD_DIM
    group_size = heads_here // kv_here
    width = out_weight.shape[1]
    paired = jnp.concatenate((key_rows, values), axis=1)
    extended = padded(paired, (("ep", 0),), WINDOW)
    offset = lax.axis_index("ep") * row_count
    seq_total = row_count * lax.axis_size("ep")
    grouped = queries.reshape(row_count, kv_here, group_size, HEAD_DIM)
    sinks = sink_logit.reshape(kv_here, group_size)[:, :, None, None]
    span_keys = QBLOCK + 2 * WINDOW

    def attend_block(block_index):
        start_row = block_index * QBLOCK
        query_block = lax.dynamic_slice_in_dim(grouped, start_row, QBLOCK, 0)
        band = lax.dynamic_slice_in_dim(extended, start_row, span_keys, 0)
        key_block = band[:, : kv_here * HEAD_DIM].reshape(span_keys, kv_here, HEAD_DIM)
        value_block = band[:, kv_here * HEAD_DIM :].reshape(span_keys, kv_here, HEAD_DIM)
        scores = jnp.einsum(
            "qhgd,khd->hgqk", query_block, key_block, preferred_element_type=jnp.float32
        ) * HEAD_DIM ** (-0.5)
        query_pos = offset + start_row + jnp.arange(QBLOCK, dtype=jnp.int32)
        key_pos = offset + start_row - WINDOW + jnp.arange(span_keys, dtype=jnp.int32)
        valid = (
            (jnp.abs(key_pos[None, :] - query_pos[:, None]) <= WINDOW)
            & (key_pos[None, :] >= 0)
            & (key_pos[None, :] < seq_total)
        )
        masked = jnp.where(valid, scores, -1e30)
        largest = jnp.maximum(jnp.max(masked, axis=-1, keepdims=True), sinks)
        raised = jnp.where(valid, jnp.exp(masked - largest), 0.0)
        denominator = jnp.sum(raised, axis=-1, keepdims=True) + jnp.exp(sinks - largest)
        weights = (raised / denominator).astype(jnp.bfloat16)
        attended = jnp.einsum(
            "hgqk,khd->qhgd", weights, value_block, preferred_element_type=jnp.float32
        )
        return attended.astype(jnp.bfloat16).reshape(QBLOCK, heads_here * HEAD_DIM)

    attended = lax.map(attend_block, jnp.arange(row_count // QBLOCK, dtype=jnp.int32))
    attended = attended.reshape(row_count, heads_here * HEAD_DIM)
    mixed = lax.psum_scatter(
        jnp.dot(attended, out_weight, preferred_element_type=jnp.float32),
        "tp",
        scatter_dimension=0,
        tiled=True,
    )
    mixer_out = (
        mixed * lax.rsqrt(jnp.mean(mixed * mixed, axis=-1, keepdims=True) + epsilon) * out_gain
    ).astype(jnp.bfloat16)
    token_total = routed_tokens.shape[0]
    inputs = routed_tokens.astype(jnp.float32)
    normed = (
        inputs
        * lax.rsqrt(jnp.mean(inputs * inputs, axis=-1, keepdims=True) + epsilon)
        * routed_gain
    ).astype(jnp.bfloat16)
    flat_ids = expert_ids.reshape(-1)
    onehot = (flat_ids[:, None] == jnp.arange(EXPERTS, dtype=jnp.int32)[None, :]).astype(jnp.int32)
    earlier = jnp.cumsum(onehot, axis=0) - onehot
    slot_index = jnp.sum(earlier * onehot, axis=1)
    flat_dest = slot_index * EXPERTS + flat_ids
    source_rows = jnp.arange(token_total * TOP, dtype=jnp.int32) // TOP
    slot_token = jnp.full((CAP * EXPERTS,), token_total, jnp.int32).at[flat_dest].set(source_rows)
    outgoing = jnp.take(normed, slot_token, axis=0, mode="fill", fill_value=0).reshape(
        1, CAP, EXPERTS, width
    )
    arrived = lax.all_to_all(outgoing, "ep", split_axis=2, concat_axis=0, tiled=True)
    source_count, slot_count, local_experts, feature_count = arrived.shape
    rows_in = arrived.reshape(source_count * slot_count, local_experts, feature_count)
    gate_piece = lax.all_gather(expert_gate, "tp", axis=2, tiled=True)
    up_piece = lax.all_gather(expert_up, "tp", axis=2, tiled=True)
    down_piece = lax.all_gather(expert_down, "tp", axis=2, tiled=True)
    gate = jnp.einsum("red,edf->ref", rows_in, gate_piece, preferred_element_type=jnp.float32)
    upward = jnp.einsum("red,edf->ref", rows_in, up_piece, preferred_element_type=jnp.float32)
    hidden = (jax.nn.silu(gate) * upward).astype(jnp.bfloat16)
    summed = jnp.einsum("ref,edf->red", hidden, down_piece, preferred_element_type=jnp.float32)
    produced = summed.astype(jnp.bfloat16).reshape(
        source_count, slot_count, local_experts, feature_count
    )
    returned = lax.all_to_all(produced, "ep", split_axis=0, concat_axis=2, tiled=True)
    returned = returned.reshape(CAP * EXPERTS, width)
    picked_rows = jnp.take(returned, flat_dest, axis=0).reshape(token_total, TOP, width)
    experts_out = jnp.sum(
        picked_rows.astype(jnp.float32) * route_weight[:, :, None], axis=1
    ).astype(jnp.bfloat16)
    return (mixer_out, experts_out)


def solution(mesh):
    placed = (
        P("ep", "tp"),
        P("ep", "tp"),
        P("ep", "tp"),
        P("tp"),
        P("tp", None),
        P(),
        P(("ep", "tp"), None),
        P(("ep", "tp"), None),
        P(("ep", "tp"), None),
        P(),
        P("ep", None, "tp"),
        P("ep", None, "tp"),
        P("ep", None, "tp"),
    )
    return jax.shard_map(
        local,
        mesh=mesh,
        in_specs=placed,
        out_specs=(P(("ep", "tp"), None), P(("ep", "tp"), None)),
        check_vma=False,
    )
```

profile of v0, /device:TPU:0, one launch (start us, length us, event | category | flops | bytes accessed | tf_op | source)
XLA Modules:
  0.0 638.6 jit_solution(18265312052773669787)
XLA Ops:
  7.2 0.7 all-gather.6.cloned.1.call-update
  8.0 0.7 all-gather.4.cloned.1.call-update
  8.7 0.7 all-gather.8.cloned.1.call-update
  9.9 0.2 reshape.268
  10.1 9.0 %reduce-window.6 = s32[32,8,128]{2,1,0:T(8,128)S(1)} reduce-window(s32[32,8,128]{2,1,0:T(8,128)S(1)} %fusion.28, s32[]{:T(128)} %constant.129.clone.1), window={size=1x1x128 pad=0_0x0_0x127_0}, to_apply=%region_6.7 | reduce-window | flops 4161536 | bytes 262148 | tf_op jit(solution)/shard_map/reduce-window
  19.7 0.6 copy-done.7
  20.3 4.3 scatter_custom_fusion
  24.8 0.5 fusion.22
  25.3 2.6 fusion.24
  27.9 11.0 %gather_fusion = bf16[2048,2048]{1,0:T(8,128)(2,1)} fusion(bf16[512,2048]{1,0:T(8,128)(2,1)S(1)} %fusion.24, s32[2048]{0:T(1024)S(1)} %fusion.29), kind=kCustom, calls=%fused_computation | custom fusion | bytes 16785408 | tf_op jit(solution)/shard_map/jit(_take)/gather | solution.py:107
  39.0 16.8 %copy_select_fusion = bf16[1,64,32,2048]{3,1,0,2:T(8,128)(2,1)} fusion(bf16[1,64,32,2048]{3,2,1,0:T(8,128)(2,1)} %bitcast.124, pred[64,32]{0,1:T(8,128)(4,1)S(1)} %copy.59), kind=kLoop, calls=%fused_computation.37 | loop fusion | flops 4194304 | bytes 16779264 | tf_op jit(solution)/shard_map/jit(_take)/select_n | solution.py:107
  55.7 7.2 %all-to-all-start = ((bf16[1,64,32,2048]{3,1,0,2:T(8,128)(2,1)}), bf16[1,64,32,2048]{3,1,0,2:T(8,128)(2,1)}, u32[]{:S(2)}, u32[]{:S(2)}) async-start(bf16[1,64,32,2048]{3,1,0,2:T(8,128)(2,1)} %copy_select_fusion), calls=%async_computation.1 | async-start | bytes 16777216 | tf_op jit(solution)/shard_map/all_to_all | solution.py:110
  63.1 3.9 collective-permute-start
  67.0 1.5 collective-permute-start.1
  68.5 1.2 copy.50
  69.7 62.0 %collective-permute-done = bf16[128,128]{0,1:T(8,128)(2,1)S(1)} collective-permute-done((bf16[128,128]{0,1:T(8,128)(2,1)S(1)}, bf16[128,128]{0,1:T(8,128)(2,1)S(1)}, u32[]{:S(2)}, u32[]{:S(2)}) %collective-permute-start) | collective-permute-done | bytes 32800 | tf_op jit(solution)/shard_map/ppermute | solution.py:20
  131.8 26.2 %while.12 = (s32[]{:T(128)}, bf16[2,512,256]{2,1,0:T(8,128)(2,1)S(1)}, s32[2]{0:T(128)S(1)}, bf16[1280,128]{0,1:T(8,128)(2,1)S(1)}, s32[]{:T(128)}, /*index=5*/b...) while((s32[]{:T(128)}, ...), condition=%wide.region_3.4_spmd, body=%wide.region_0.3_spmd.sunk | while | flops 426778112 | bytes 47478104 | solution.py:82
  131.8 0.6 dynamic_slice.28
  133.1 0.8 fusion.54
  133.9 1.2 fusion.55
  135.2 3.1 copy-done.2
  138.3 1.6 fusion.56
  140.0 5.0 fusion.57
  145.2 0.6 dynamic_slice.28
  146.5 0.8 fusion.54
  147.3 1.2 fusion.55
  148.6 2.6 copy-done.2
  151.2 1.6 fusion.56
  152.8 5.0 fusion.57
  158.1 4.5 fusion.37
  162.6 83.9 %all-to-all-done = bf16[1,64,32,2048]{3,1,0,2:T(8,128)(2,1)} async-done(((bf16[1,64,32,2048]{3,1,0,2:T(8,128)(2,1)}), bf16[1,64,32,2048]{3,1,0,2:T(8,128)(2,1)}, u32[]{:S(2)}, u32[]{:S(2)}) %all-to-all-start) | async-done | bytes 8388640 | tf_op jit(solution)/shard_map/all_to_all | solution.py:110
  246.5 8.9 %copy.61 = bf16[8,1,64,4,2048]{4,2,0,3,1:T(8,128)(2,1)} copy(bf16[8,1,64,4,2048]{4,2,3,0,1:T(8,128)(2,1)} %bitcast.20) | data formatting | bytes 16777216 | tf_op jit(solution)/shard_map/all_to_all | solution.py:110
  255.4 17.1 %fusion.38 = f32[4,512,1024]{2,1,0:T(8,128)} fusion(bf16[512,4,2048]{2,0,1:T(8,128)(2,1)} %bitcast.125, bf16[4,2048,1024]{2,1,0:T(8,128)(2,1)} %all-gather.6.cloned.1.call-done), kind=kOutput, calls=%fused_computation.81 | convolution fusion | flops 8589934592 | bytes 33554432 | tf_op jit(solution)/shard_map/red,edf->ref/dot_general | solution.py:117
  272.5 67.5 %all-gather.8.cloned.1.call-done = bf16[4,2048,1024]{2,1,0:T(8,128)(2,1)} async-done(((bf16[4,2048,256]{2,1,0:T(8,128)(2,1)}), bf16[4,2048,1024]{2,1,0:T(8,128)(2,1)}) %all-gather.8.cloned.1.call-update) | async-done | bytes 16777232 | tf_op jit(solution)/shard_map/all_gather | solution.py:115
  340.0 28.9 %convolution_convert_fusion = bf16[4,512,2048]{2,1,0:T(8,128)(2,1)} fusion(bf16[4,2048,1024]{2,1,0:T(8,128)(2,1)} %all-gather.8.cloned.1.call-done, f32[4,512,1024]{2,1,0:T(8,128)} %fusion.38, bf16[512,4,2048]{2,0,1:T(8,128)(2,1)} %bitcast.126, bf16[4,2048,1024]{2,1,0:T(8,128)(2,1)} %all-gather.4.cloned.1.call-done), kind=kOutput, calls=%fused_computation.40 | convolution fusion | flops 17196646400 | bytes 58720256 | tf_op jit(solution)/shard_map/ref,edf->red/dot_general | solution.py:119
  368.9 8.3 %copy.62 = bf16[8,64,4,2048]{3,1,2,0:T(8,128)(2,1)} copy(bf16[8,64,4,2048]{3,1,0,2:T(8,128)(2,1)} %bitcast.127) | data formatting | bytes 16777216 | tf_op jit(solution)/shard_map/reshape | solution.py:120
  377.2 5.7 all-to-all-start.1
  382.9 0.2 mul.111
  383.2 0.2 copy.57
  383.6 30.2 %reduce-scatter.2.cloned.1.call-done = f32[256,2048]{1,0:T(8,128)} async-done(((f32[1024,2048]{1,0:T(8,128)}), f32[256,2048]{1,0:T(8,128)}) %reduce-scatter.2.cloned.1.call-update) | async-done | bytes 2097168 | tf_op jit(solution)/shard_map/reduce_scatter | solution.py:84
  413.8 1.8 multiply_reduce_fusion.1
  415.7 2.8 multiply_convert_fusion
  418.5 147.9 %all-to-all-done.1 = bf16[8,64,4,2048]{3,1,2,0:T(8,128)(2,1)} async-done(((bf16[8,64,4,2048]{3,1,2,0:T(8,128)(2,1)}), bf16[8,64,4,2048]{3,1,2,0:T(8,128)(2,1)}, u32[]{:S(2)}, u32[]{:S(2)}) %all-to-all-start.1) | async-done | bytes 8388640 | tf_op jit(solution)/shard_map/all_to_all | solution.py:123
  566.4 12.1 %copy.63 = bf16[1,64,8,4,2048]{4,3,2,1,0:T(4,128)(2,1)} copy(bf16[1,64,8,4,2048]{4,1,3,2,0:T(8,128)(2,1)} %bitcast.27) | data formatting | bytes 16777216 | tf_op jit(solution)/shard_map/all_to_all | solution.py:123
  578.5 12.5 %reshape.271 = bf16[2048,2048]{1,0:T(8,128)(2,1)} reshape(bf16[1,64,8,4,2048]{4,3,2,1,0:T(4,128)(2,1)} %copy.63) | data formatting | bytes 16777216 | tf_op jit(solution)/shard_map/reshape | solution.py:124
  591.0 13.4 %gather_fusion.1 = bf16[1024,2048]{1,0:T(8,128)(2,1)} fusion(bf16[2048,2048]{1,0:T(8,128)(2,1)} %reshape.271, s32[1024]{0:T(1024)S(1)} %broadcast_clamp_fusion), kind=kCustom, calls=%fused_computation.1 | custom fusion | bytes 8392704 | tf_op jit(solution)/shard_map/jit(_take)/gather | solution.py:125
  604.4 7.6 %gather.15 = bf16[512,2,2048]{2,1,0:T(2,128)(2,1)} reshape(bf16[1024,2048]{1,0:T(8,128)(2,1)} %gather_fusion.1) | data formatting | bytes 8388608 | tf_op jit(solution)/shard_map/jit(_take)/gather | solution.py:125
  612.0 20.0 %multiply_reduce_fusion = bf16[512,2048]{1,0:T(8,128)(2,1)} fusion(bf16[512,2,2048]{2,1,0:T(2,128)(2,1)} %gather.15, pred[512,2]{1,0:T(8,128)(4,1)S(1)} %copy.57, f32[512,2]{1,0:T(8,128)S(1)} %copy.64), kind=kLoop, calls=%fused_computation.38 | loop fusion | flops 7340032 | bytes 6296576 | tf_op jit(solution)/shard_map/reduce_sum | solution.py:126
  (83 shorter events, 2.4 us)
Async XLA Ops:
  7.2 150.9 %copy-start = (bf16[256,2048]{1,0:T(8,128)(2,1)S(1)}, bf16[256,2048]{1,0:T(8,128)(2,1)}, u32[]{:S(2)}) copy-start(bf16[256,2048]{1,0:T(8,128)(2,1)} %param.19) | copy-start | bytes 3145732
  7.2 2.3 copy-start.9
  7.2 248.2 %all-gather.6.cloned.1.call-start = ((), (), s32[]{:S(2)}) async-start(), calls=%async_computation.5 | async-start | bytes 20971520 | tf_op jit(solution)/shard_map/all_gather | solution.py:114
  7.9 16.9 %copy-start.3 = (bf16[512,2048]{1,0:T(8,128)(2,1)S(1)}, bf16[512,2048]{1,0:T(8,128)(2,1)}, u32[]{:S(2)}) copy-start(bf16[512,2048]{1,0:T(8,128)(2,1)} %param.21) | copy-start | bytes 6291460
  7.9 17.4 %copy-start.13 = (f32[2048]{0:T(1024)S(1)}, f32[2048]{0:T(1024)}, u32[]{:S(2)}) copy-start(f32[2048]{0:T(1024)} %param.24) | copy-start | bytes 24580
  7.9 264.5 %all-gather.4.cloned.1.call-start = ((), (), s32[]{:S(2)}) async-start(), calls=%async_computation.4 | async-start | bytes 20971520 | tf_op jit(solution)/shard_map/all_gather | solution.py:113
  8.7 331.3 %all-gather.8.cloned.1.call-start = ((), (), s32[]{:S(2)}) async-start(), calls=%async_computation.6 | async-start | bytes 20971520 | tf_op jit(solution)/shard_map/all_gather | solution.py:115
  19.7 0.6 copy-start.7
  20.3 4.3 copy-start.11
  55.7 7.3 %copy-start.4 = (bf16[1024,64]{0,1:T(8,128)(2,1)S(1)}, bf16[1024,64]{0,1:T(8,128)(2,1)}, u32[]{:S(2)}) copy-start(bf16[1024,64]{0,1:T(8,128)(2,1)} %param.16) | copy-start | bytes 393220
  55.7 7.3 %copy-start.5 = (bf16[1024,64]{0,1:T(8,128)(2,1)S(1)}, bf16[1024,64]{0,1:T(8,128)(2,1)}, u32[]{:S(2)}) copy-start(bf16[1024,64]{0,1:T(8,128)(2,1)} %param.17) | copy-start | bytes 393220
  55.7 76.1 %copy-start.6 = (f32[4]{0:T(128)S(1)}, f32[4]{0:T(128)}, u32[]{:S(2)}) copy-start(f32[4]{0:T(128)} %param.18) | copy-start | bytes 52
  55.7 190.7 %all-to-all-start = ((bf16[1,64,32,2048]{3,1,0,2:T(8,128)(2,1)}), bf16[1,64,32,2048]{3,1,0,2:T(8,128)(2,1)}, u32[]{:S(2)}, u32[]{:S(2)}) async-start(bf16[1,64,32,2048]{3,1,0,2:T(8,128)(2,1)} %copy_select_fusion), calls=%async_computation.1 | async-start | bytes 16777216 | tf_op jit(solution)/shard_map/all_to_all | solution.py:110
  63.0 350.9 %reduce-scatter.2.cloned.1.call-start = ((), (), s32[]{:S(2)}) async-start(), calls=%async_computation.3 | async-start | bytes 10485760 | tf_op jit(solution)/shard_map/reduce_scatter | solution.py:84
  63.1 68.7 %collective-permute-start = (bf16[128,128]{0,1:T(8,128)(2,1)S(1)}, bf16[128,128]{0,1:T(8,128)(2,1)S(1)}, u32[]{:S(2)}, u32[]{:S(2)}) collective-permute-start(bf16[128,128]{0,1:T(8,128)(2,1)S(1)} %get-tuple-element.110), channel_id=1, source_target_pairs={{0,4},{4,8},{8,12},{12,16},{16,20},{20,24},{24,28},{1,5},{5,9},{9,... | collective-permute-start | bytes 98312 | tf_op jit(solution)/shard_map/ppermute | solution.py:20
  67.0 64.8 %collective-permute-start.1 = (bf16[128,128]{0,1:T(8,128)(2,1)S(1)}, bf16[128,128]{0,1:T(8,128)(2,1)S(1)}, u32[]{:S(2)}, u32[]{:S(2)}) collective-permute-start(bf16[128,128]{0,1:T(8,128)(2,1)S(1)} %get-tuple-element.111), channel_id=1, source_target_pairs={{4,0},{8,4},{12,8},{16,12},{20,16},{24,20},{28,24},{5,1},{9,5},{13... | collective-permute-start | bytes 98312 | tf_op jit(solution)/shard_map/ppermute | solution.py:23
  135.1 3.2 copy-start.2
  148.5 2.7 copy-start.2
  377.1 5.8 copy-start.8
  377.1 6.1 copy-start.10
  377.1 6.3 copy-start.15
  377.1 6.5 %copy-start.12 = (s32[1024,1]{0,1:T(1,128)S(1)}, s32[1024,1]{0,1:T(1,128)}, u32[]{:S(2)}) copy-start(s32[1024,1]{0,1:T(1,128)} %copy-done.11) | copy-start | bytes 12292
  377.1 38.5 %copy-start.14 = (f32[2048]{0:T(1024)S(1)}, f32[2048]{0:T(1024)}, u32[]{:S(2)}) copy-start(f32[2048]{0:T(1024)} %param.20) | copy-start | bytes 24580
  377.2 189.2 %all-to-all-start.1 = ((bf16[8,64,4,2048]{3,1,2,0:T(8,128)(2,1)}), bf16[8,64,4,2048]{3,1,2,0:T(8,128)(2,1)}, u32[]{:S(2)}, u32[]{:S(2)}) async-start(bf16[8,64,4,2048]{3,1,2,0:T(8,128)(2,1)} %copy.62), calls=%async_computation.2 | async-start | bytes 16777216 | tf_op jit(solution)/shard_map/all_to_all | solution.py:123
  591.0 41.0 %copy-start.1 = (bf16[256,2048]{1,0:T(8,128)(2,1)S(1)}, bf16[256,2048]{1,0:T(8,128)(2,1)}, u32[]{:S(2)}) copy-start(bf16[256,2048]{1,0:T(8,128)(2,1)} %param.19) | copy-start | bytes 3145732
Sparse Core Ops, SparseCore 0:
  9.5 110.8 all-gather.5
  122.0 108.1 all-gather.3
  231.8 108.1 all-gather.7
  342.4 71.4 reduce-scatter.1
where the time goes:
time: 640 us; the launch traced here: 639 us
  waiting for transfers between devices  394 us (62%)
  local copies, waits for them, and re-layouts  89 us (14%)
  matrix products  63 us (10%)
  other arithmetic  58.9 us (9%)
  starting transfers between devices  18.5 us (3%)
  between operations  14.1 us (2%)
    all_to_all x1, waiting for transfers between devices, local(): lax.all_to_all(produced, 'ep', split_axis=0, concat_axis=2, tiled=True)  148 us
    all_to_all x1, waiting for transfers between devices, local(): lax.all_to_all(outgoing, 'ep', split_axis=2, concat_axis=0, tiled=True)  83.9 us
    all_gather x1, waiting for transfers between devices, local(): down_piece = lax.all_gather(expert_down, 'tp', axis=2, tiled=True)  67.5 us
    ppermute x1, waiting for transfers between devices, padded(): lax.ppermute(lax.slice_in_dim(block, block.shape[dim] - width, None, axis...  62 us
    reduce_scatter x1, waiting for transfers between devices, local(): lax.psum_scatter(jnp.dot(attended, out_weight, preferred_element_type=jnp...  30.2 us
    dot_general x1, matrix products, local(): jnp.einsum('ref,edf->red', hidden, down_piece, preferred_element_type=jnp...  28.9 us
    gather x2, local copies, waits for them, and re-layouts, local(): jnp.take(returned, flat_dest, axis=0).reshape(token_total, TOP, width)  21 us
    reduce_sum x1, other arithmetic, local(): jnp.sum(picked_rows.astype(jnp.float32) * route_weight[:, :, None], axis=1)  20 us
  transfers between devices with their start and end apart: 8, of which 5 were waited for; matrix products, arithmetic and copies ran while one was open for 22% of the time, Pallas kernels for 0%

commit v1 on v0

--- a/solution.py
+++ b/solution.py
@@ -10,6 +10,22 @@
 TOP = 2
 CAP = 64
 epsilon = 1e-06
+
+
+def ring_product(value, axis, dim, contribution):
+    size, index, width = (lax.axis_size(axis), lax.axis_index(axis), value.shape[dim])
+    upward = [(i, (i + 1) % size) for i in range(size)]
+    left = [(i, (i - 1) % size) for i in range(size)]
+    halfway = size // 2
+    from_left = from_right = value
+    total = contribution(value, index * width)
+    for step in range(1, halfway + 1):
+        from_left = lax.ppermute(from_left, axis, upward)
+        if step < size - halfway:
+            from_right = lax.ppermute(from_right, axis, left)
+            total = total + contribution(from_right, (index + step) % size * width)
+        total = total + contribution(from_left, (index - step) % size * width)
+    return total
 
 
 def padded(block, sides, width):
@@ -112,11 +128,20 @@
     rows_in = arrived.reshape(source_count * slot_count, local_experts, feature_count)
     gate_piece = lax.all_gather(expert_gate, "tp", axis=2, tiled=True)
     up_piece = lax.all_gather(expert_up, "tp", axis=2, tiled=True)
-    down_piece = lax.all_gather(expert_down, "tp", axis=2, tiled=True)
     gate = jnp.einsum("red,edf->ref", rows_in, gate_piece, preferred_element_type=jnp.float32)
     upward = jnp.einsum("red,edf->ref", rows_in, up_piece, preferred_element_type=jnp.float32)
     hidden = (jax.nn.silu(gate) * upward).astype(jnp.bfloat16)
-    summed = jnp.einsum("ref,edf->red", hidden, down_piece, preferred_element_type=jnp.float32)
+    summed = ring_product(
+        expert_down,
+        "tp",
+        2,
+        lambda own_block, offset_2: jnp.einsum(
+            "ref,edf->red",
+            lax.dynamic_slice_in_dim(hidden, offset_2, own_block.shape[2], axis=2),
+            own_block,
+            preferred_element_type=jnp.float32,
+        ),
+    )
     produced = summed.astype(jnp.bfloat16).reshape(
         source_count, slot_count, local_experts, feature_count
     )

time: 640 us -> 678 us (1.059)
  matrix products: 63 us -> 104 us
  waiting for transfers between devices: 394 us -> 385 us
    ppermute x0 -> x3, waiting for transfers between devices: none -> 70.9 us  [the longest x2 70.9 us: ring_product(): from_left = lax.ppermute(from_left, axis, upward)]
    all_to_all x1, waiting for transfers between devices: 83.9 us -> 13.4 us  [local(): lax.all_to_all(outgoing, 'ep', split_axis=2, concat_axis=0, tiled=True)]
    all_gather x1 -> x0, waiting for transfers between devices: 67.5 us -> none  [local(): down_piece = lax.all_gather(expert_down, 'tp', axis=2, tiled=True)]
    all_gather x1, waiting for transfers between devices: 0.01 us -> 59.4 us  [local(): gate_piece = lax.all_gather(expert_gate, 'tp', axis=2, tiled=True)]
    dot_general x1 -> x5, matrix products: 28.9 us -> 70.6 us  [the longest x4 52 us: local(): jnp.einsum('ref,edf->red', lax.dynamic_slice_in_dim(hidden, offset_2, own...]
    all_to_all x1, waiting for transfers between devices: 148 us -> 178 us  [local(): lax.all_to_all(produced, 'ep', split_axis=0, concat_axis=2, tiled=True)]
    reduce_scatter x1, waiting for transfers between devices: 30.2 us -> 0.02 us  [local(): lax.psum_scatter(jnp.dot(attended, out_weight, preferred_element_type=jnp...]
  transfers between devices with their start and end apart: 8 -> 10, of which waited for: 5 -> 5; matrix products, arithmetic and copies ran while one was open for 22% -> 27% of each run, Pallas kernels for 0% -> 0%
where the time goes in v1:
time: 678 us; the launch traced here: 671 us
  waiting for transfers between devices  385 us (57%)
  matrix products  104 us (15%)
  local copies, waits for them, and re-layouts  87.7 us (13%)
  other arithmetic  58.9 us (9%)
  starting transfers between devices  19.5 us (3%)
  between operations  14.4 us (2%)
    all_to_all x1, waiting for transfers between devices, local(): lax.all_to_all(produced, 'ep', split_axis=0, concat_axis=2, tiled=True)  178 us
    ppermute x2, waiting for transfers between devices, ring_product(): from_left = lax.ppermute(from_left, axis, upward)  70.9 us
    ppermute x1, waiting for transfers between devices, padded(): lax.ppermute(lax.slice_in_dim(block, block.shape[dim] - width, None, axis...  61.4 us
    all_gather x1, waiting for transfers between devices, local(): gate_piece = lax.all_gather(expert_gate, 'tp', axis=2, tiled=True)  59.4 us
    dot_general x4, matrix products, local(): jnp.einsum('ref,edf->red', lax.dynamic_slice_in_dim(hidden, offset_2, own...  52 us
    gather x2, local copies, waits for them, and re-layouts, local(): jnp.take(returned, flat_dest, axis=0).reshape(token_total, TOP, width)  21 us
    reduce_sum x1, other arithmetic, local(): jnp.sum(picked_rows.astype(jnp.float32) * route_weight[:, :, None], axis=1)  20 us
    dot_general x1, matrix products, local(): jnp.einsum('red,edf->ref', rows_in, gate_piece, preferred_element_type=jn...  18.6 us
  transfers between devices with their start and end apart: 10, of which 5 were waited for; matrix products, arithmetic and copies ran while one was open for 27% of the time, Pallas kernels for 0%

profile of v1, /device:TPU:0, one launch (start us, length us, event | category | flops | bytes accessed | tf_op | source)
XLA Modules:
  0.0 670.9 jit_solution(5561233337844783146)
XLA Ops:
  7.3 0.7 all-gather.5.cloned.1.call-update
  8.0 0.7 all-gather.3.cloned.1.call-update
  9.4 9.0 %reduce-window.6 = s32[32,8,128]{2,1,0:T(8,128)S(1)} reduce-window(s32[32,8,128]{2,1,0:T(8,128)S(1)} %fusion.35, s32[]{:T(128)} %constant.153.clone.1), window={size=1x1x128 pad=0_0x0_0x127_0}, to_apply=%region_6.7 | reduce-window | flops 4161536 | bytes 262148 | tf_op jit(solution)/shard_map/reduce-window
  19.0 0.6 copy-done.9
  19.5 4.3 scatter_custom_fusion
  24.6 2.7 fusion.24
  27.3 11.0 %gather_fusion = bf16[2048,2048]{1,0:T(8,128)(2,1)} fusion(bf16[512,2048]{1,0:T(8,128)(2,1)S(1)} %fusion.24, s32[2048]{0:T(1024)S(1)} %fusion.36), kind=kCustom, calls=%fused_computation | custom fusion | bytes 16785408 | tf_op jit(solution)/shard_map/jit(_take)/gather | solution.py:123
  38.3 16.8 %copy_select_fusion = bf16[1,64,32,2048]{3,1,0,2:T(8,128)(2,1)} fusion(bf16[1,64,32,2048]{3,2,1,0:T(8,128)(2,1)} %bitcast.123, pred[64,32]{0,1:T(8,128)(4,1)S(1)} %copy.59), kind=kLoop, calls=%fused_computation.38 | loop fusion | flops 4194304 | bytes 16779264 | tf_op jit(solution)/shard_map/jit(_take)/select_n | solution.py:123
  55.1 7.3 %all-to-all-start = ((bf16[1,64,32,2048]{3,1,0,2:T(8,128)(2,1)}), bf16[1,64,32,2048]{3,1,0,2:T(8,128)(2,1)}, u32[]{:S(2)}, u32[]{:S(2)}) async-start(bf16[1,64,32,2048]{3,1,0,2:T(8,128)(2,1)} %copy_select_fusion), calls=%async_computation.1 | async-start | bytes 16777216 | tf_op jit(solution)/shard_map/all_to_all | solution.py:126
  62.5 3.9 collective-permute-start
  66.4 1.3 collective-permute-start.1
  67.8 0.7 collective-permute-start.3
  68.5 1.2 copy.50
  69.8 61.4 %collective-permute-done = bf16[128,128]{0,1:T(8,128)(2,1)S(1)} collective-permute-done((bf16[128,128]{0,1:T(8,128)(2,1)S(1)}, bf16[128,128]{0,1:T(8,128)(2,1)S(1)}, u32[]{:S(2)}, u32[]{:S(2)}) %collective-permute-start) | collective-permute-done | bytes 32800 | tf_op jit(solution)/shard_map/ppermute | solution.py:36
  131.2 25.3 %while.12 = (s32[]{:T(128)}, bf16[2,512,256]{2,1,0:T(8,128)(2,1)S(1)}, s32[2]{0:T(128)S(1)}, bf16[1280,128]{0,1:T(8,128)(2,1)S(1)}, s32[]{:T(128)}, /*index=5*/b...) while((s32[]{:T(128)}, ...), condition=%wide.region_3.4_spmd, body=%wide.region_0.3_spmd.sunk | while | flops 426778112 | bytes 47478104 | solution.py:98
  131.2 0.6 dynamic_slice.52
  132.5 0.8 fusion.67
  133.3 1.2 fusion.68
  134.6 2.5 copy-done.2
  137.1 1.6 fusion.69
  138.8 4.9 fusion.70
  143.9 0.6 dynamic_slice.52
  145.2 0.8 fusion.67
  146.0 1.2 fusion.68
  147.3 2.5 copy-done.2
  149.8 1.6 fusion.69
  151.4 4.9 fusion.70
  156.5 4.5 fusion.47
  161.1 70.9 %collective-permute-done.3 = bf16[4,2048,256]{2,1,0:T(8,128)(2,1)} collective-permute-done((bf16[4,2048,256]{2,1,0:T(8,128)(2,1)}, bf16[4,2048,256]{2,1,0:T(8,128)(2,1)}, u32[]{:S(2)}, u32[]{:S(2)}) %collective-permute-start.3) | collective-permute-done | bytes 4194336 | tf_op jit(solution)/shard_map/ppermute | solution.py:23
  232.5 13.4 %all-to-all-done = bf16[1,64,32,2048]{3,1,0,2:T(8,128)(2,1)} async-done(((bf16[1,64,32,2048]{3,1,0,2:T(8,128)(2,1)}), bf16[1,64,32,2048]{3,1,0,2:T(8,128)(2,1)}, u32[]{:S(2)}, u32[]{:S(2)}) %all-to-all-start) | async-done | bytes 8388640 | tf_op jit(solution)/shard_map/all_to_all | solution.py:126
  245.9 8.3 %copy.61 = bf16[8,1,64,4,2048]{4,2,0,3,1:T(8,128)(2,1)} copy(bf16[8,1,64,4,2048]{4,2,3,0,1:T(8,128)(2,1)} %bitcast.20) | data formatting | bytes 16777216 | tf_op jit(solution)/shard_map/all_to_all | solution.py:126
  254.2 16.8 %fusion.48 = f32[4,512,1024]{2,1,0:T(8,128)} fusion(bf16[512,4,2048]{2,0,1:T(8,128)(2,1)} %bitcast.125, bf16[4,2048,1024]{2,1,0:T(8,128)(2,1)} %all-gather.5.cloned.1.call-done), kind=kOutput, calls=%fused_computation.91 | convolution fusion | flops 8589934592 | bytes 33554432 | tf_op jit(solution)/shard_map/red,edf->ref/dot_general | solution.py:132
  271.0 59.4 %all-gather.3.cloned.1.call-done = bf16[4,2048,1024]{2,1,0:T(8,128)(2,1)} async-done(((bf16[4,2048,256]{2,1,0:T(8,128)(2,1)}), bf16[4,2048,1024]{2,1,0:T(8,128)(2,1)}) %all-gather.3.cloned.1.call-update) | async-done | bytes 16777232 | tf_op jit(solution)/shard_map/all_gather | solution.py:129
  330.4 18.6 %fusion.18 = bf16[512,4,1024]{2,0,1:T(8,128)(2,1)S(1)} fusion(f32[4,512,1024]{2,1,0:T(8,128)} %fusion.48, bf16[512,4,2048]{2,0,1:T(8,128)(2,1)} %bitcast.126, bf16[4,2048,1024]{2,1,0:T(8,128)(2,1)} %all-gather.3.cloned.1.call-done), kind=kOutput, calls=%fused_computation.32 | convolution fusion | flops 8602517504 | bytes 37748736 | tf_op jit(solution)/shard_map/red,edf->ref/dot_general | solution.py:131
  349.0 8.6 %fusion.30 = f32[4,512,2048]{2,1,0:T(8,128)} fusion(bf16[4,2048,256]{2,1,0:T(8,128)(2,1)S(1)} %copy-done.5, bf16[512,4,1024]{2,0,1:T(8,128)(2,1)S(1)} %fusion.18, s32[]{:T(128)S(6)} %select_n.100), kind=kOutput, calls=%fused_computation.53 | convolution fusion | flops 2147483648 | bytes 22020100 | tf_op jit(solution)/shard_map/ref,edf->red/dot_general | solution.py:138
  357.6 10.4 %fusion.26 = f32[4,512,2048]{2,1,0:T(8,128)} fusion(bf16[4,2048,256]{2,1,0:T(8,128)(2,1)} %collective-permute-done.3, bf16[512,4,1024]{2,0,1:T(8,128)(2,1)S(1)} %fusion.18, s32[]{:T(128)S(6)} %select_n.104), kind=kOutput, calls=%fused_computation.49 | convolution fusion | flops 2147483648 | bytes 22020100 | tf_op jit(solution)/shard_map/ref,edf->red/dot_general | solution.py:138
  368.0 10.4 %fusion.28 = f32[4,512,2048]{2,1,0:T(8,128)} fusion(bf16[4,2048,256]{2,1,0:T(8,128)(2,1)} %collective-permute-done.2, bf16[512,4,1024]{2,0,1:T(8,128)(2,1)S(1)} %fusion.18, s32[]{:T(128)S(6)} %select_n.102), kind=kOutput, calls=%fused_computation.51 | convolution fusion | flops 2147483648 | bytes 22020100 | tf_op jit(solution)/shard_map/ref,edf->red/dot_general | solution.py:138
  378.4 22.5 %add_convert_fusion = bf16[4,512,2048]{2,1,0:T(8,128)(2,1)} fusion(f32[4,512,2048]{2,1,0:T(8,128)} %fusion.26, f32[4,512,2048]{2,1,0:T(8,128)} %fusion.30, f32[4,512,2048]{2,1,0:T(8,128)} %fusion.28, bf16[4,2048,256]{2,1,0:T(8,128)(2,1)} %collective-permute-done.4, bf16[512,4,1024]{2,0,1:T(8,128)(2,1)} %copy-done.4, s32[]{:T(128)S(6)} %select_n.106), kind=kOutput, calls=%fused_computation.30 | convolution fusion | flops 2164260864 | bytes 63963140 | tf_op jit(solution)/shard_map/ref,edf->red/dot_general | solution.py:138
  401.0 8.3 %copy.62 = bf16[8,64,4,2048]{3,1,2,0:T(8,128)(2,1)} copy(bf16[8,64,4,2048]{3,1,0,2:T(8,128)(2,1)} %bitcast.124) | data formatting | bytes 16777216 | tf_op jit(solution)/shard_map/reshape | solution.py:145
  409.3 5.6 all-to-all-start.1
  415.6 1.8 multiply_reduce_fusion.1
  417.5 2.8 multiply_convert_fusion
  420.3 178.2 %all-to-all-done.1 = bf16[8,64,4,2048]{3,1,2,0:T(8,128)(2,1)} async-done(((bf16[8,64,4,2048]{3,1,2,0:T(8,128)(2,1)}), bf16[8,64,4,2048]{3,1,2,0:T(8,128)(2,1)}, u32[]{:S(2)}, u32[]{:S(2)}) %all-to-all-start.1) | async-done | bytes 8388640 | tf_op jit(solution)/shard_map/all_to_all | solution.py:148
  598.5 12.1 %copy.63 = bf16[1,64,8,4,2048]{4,3,2,1,0:T(4,128)(2,1)} copy(bf16[1,64,8,4,2048]{4,1,3,2,0:T(8,128)(2,1)} %bitcast.27) | data formatting | bytes 16777216 | tf_op jit(solution)/shard_map/all_to_all | solution.py:148
  610.6 12.5 %reshape.271 = bf16[2048,2048]{1,0:T(8,128)(2,1)} reshape(bf16[1,64,8,4,2048]{4,3,2,1,0:T(4,128)(2,1)} %copy.63) | data formatting | bytes 16777216 | tf_op jit(solution)/shard_map/reshape | solution.py:149
  623.1 13.4 %gather_fusion.1 = bf16[1024,2048]{1,0:T(8,128)(2,1)} fusion(bf16[2048,2048]{1,0:T(8,128)(2,1)} %reshape.271, s32[1024]{0:T(1024)S(1)} %broadcast_clamp_fusion), kind=kCustom, calls=%fused_computation.1 | custom fusion | bytes 8392704 | tf_op jit(solution)/shard_map/jit(_take)/gather | solution.py:150
  636.5 7.6 %gather.15 = bf16[512,2,2048]{2,1,0:T(2,128)(2,1)} reshape(bf16[1024,2048]{1,0:T(8,128)(2,1)} %gather_fusion.1) | data formatting | bytes 8388608 | tf_op jit(solution)/shard_map/jit(_take)/gather | solution.py:150
  644.1 20.0 %multiply_reduce_fusion = bf16[512,2048]{1,0:T(8,128)(2,1)} fusion(bf16[512,2,2048]{2,1,0:T(2,128)(2,1)} %gather.15, pred[512,2]{1,0:T(8,128)(4,1)S(1)} %copy.57, f32[512,2]{1,0:T(8,128)S(1)} %copy.64), kind=kLoop, calls=%fused_computation.39 | loop fusion | flops 7340032 | bytes 6296576 | tf_op jit(solution)/shard_map/reduce_sum | solution.py:151
  (94 shorter events, 4.1 us)
Async XLA Ops:
  7.2 149.4 %copy-start = (bf16[256,2048]{1,0:T(8,128)(2,1)S(1)}, bf16[256,2048]{1,0:T(8,128)(2,1)}, u32[]{:S(2)}) copy-start(bf16[256,2048]{1,0:T(8,128)(2,1)} %param.19) | copy-start | bytes 3145732
  7.2 1.5 copy-start.11
  7.2 16.9 %copy-start.3 = (bf16[512,2048]{1,0:T(8,128)(2,1)S(1)}, bf16[512,2048]{1,0:T(8,128)(2,1)}, u32[]{:S(2)}) copy-start(bf16[512,2048]{1,0:T(8,128)(2,1)} %param.21) | copy-start | bytes 6291460
  7.2 17.4 %copy-start.15 = (f32[2048]{0:T(1024)S(1)}, f32[2048]{0:T(1024)}, u32[]{:S(2)}) copy-start(f32[2048]{0:T(1024)} %param.24) | copy-start | bytes 24580
  7.2 247.0 %all-gather.5.cloned.1.call-start = ((), (), s32[]{:S(2)}) async-start(), calls=%async_computation.5 | async-start | bytes 20971520 | tf_op jit(solution)/shard_map/all_gather | solution.py:130
  7.9 322.4 %all-gather.3.cloned.1.call-start = ((), (), s32[]{:S(2)}) async-start(), calls=%async_computation.4 | async-start | bytes 20971520 | tf_op jit(solution)/shard_map/all_gather | solution.py:129
  18.9 0.6 copy-start.9
  19.5 4.3 copy-start.13
  55.1 7.3 %copy-start.6 = (bf16[1024,64]{0,1:T(8,128)(2,1)S(1)}, bf16[1024,64]{0,1:T(8,128)(2,1)}, u32[]{:S(2)}) copy-start(bf16[1024,64]{0,1:T(8,128)(2,1)} %param.16) | copy-start | bytes 393220
  55.1 7.3 %copy-start.7 = (bf16[1024,64]{0,1:T(8,128)(2,1)S(1)}, bf16[1024,64]{0,1:T(8,128)(2,1)}, u32[]{:S(2)}) copy-start(bf16[1024,64]{0,1:T(8,128)(2,1)} %param.17) | copy-start | bytes 393220
  55.1 76.1 %copy-start.8 = (f32[4]{0:T(128)S(1)}, f32[4]{0:T(128)}, u32[]{:S(2)}) copy-start(f32[4]{0:T(128)} %param.18) | copy-start | bytes 52
  55.1 190.8 %all-to-all-start = ((bf16[1,64,32,2048]{3,1,0,2:T(8,128)(2,1)}), bf16[1,64,32,2048]{3,1,0,2:T(8,128)(2,1)}, u32[]{:S(2)}, u32[]{:S(2)}) async-start(bf16[1,64,32,2048]{3,1,0,2:T(8,128)(2,1)} %copy_select_fusion), calls=%async_computation.1 | async-start | bytes 16777216 | tf_op jit(solution)/shard_map/all_to_all | solution.py:126
  62.4 353.3 %reduce-scatter.2.cloned.1.call-start = ((), (), s32[]{:S(2)}) async-start(), calls=%async_computation.3 | async-start | bytes 10485760 | tf_op jit(solution)/shard_map/reduce_scatter | solution.py:100
  62.5 68.7 %collective-permute-start = (bf16[128,128]{0,1:T(8,128)(2,1)S(1)}, bf16[128,128]{0,1:T(8,128)(2,1)S(1)}, u32[]{:S(2)}, u32[]{:S(2)}) collective-permute-start(bf16[128,128]{0,1:T(8,128)(2,1)S(1)} %get-tuple-element.110), channel_id=1, source_target_pairs={{0,4},{4,8},{8,12},{12,16},{16,20},{20,24},{24,28},{1,5},{5,9},{9,... | collective-permute-start | bytes 98312 | tf_op jit(solution)/shard_map/ppermute | solution.py:36
  66.4 64.8 %collective-permute-start.1 = (bf16[128,128]{0,1:T(8,128)(2,1)S(1)}, bf16[128,128]{0,1:T(8,128)(2,1)S(1)}, u32[]{:S(2)}, u32[]{:S(2)}) collective-permute-start(bf16[128,128]{0,1:T(8,128)(2,1)S(1)} %get-tuple-element.111), channel_id=1, source_target_pairs={{4,0},{8,4},{12,8},{16,12},{20,16},{24,20},{28,24},{5,1},{9,5},{13... | collective-permute-start | bytes 98312 | tf_op jit(solution)/shard_map/ppermute | solution.py:39
  67.7 300.4 %collective-permute-start.2 = (bf16[4,2048,256]{2,1,0:T(8,128)(2,1)}, bf16[4,2048,256]{2,1,0:T(8,128)(2,1)}, u32[]{:S(2)}, u32[]{:S(2)}) collective-permute-start(bf16[4,2048,256]{2,1,0:T(8,128)(2,1)} %param.27), channel_id=1, source_target_pairs={{0,3},{1,0},{2,1},{3,2},{4,7},{5,4},{6,5},{7,6},{8,11},{9,8},{10,9... | collective-permute-start | bytes 12582920 | tf_op jit(solution)/shard_map/ppermute | solution.py:25
  67.8 164.1 %collective-permute-start.3 = (bf16[4,2048,256]{2,1,0:T(8,128)(2,1)}, bf16[4,2048,256]{2,1,0:T(8,128)(2,1)}, u32[]{:S(2)}, u32[]{:S(2)}) collective-permute-start(bf16[4,2048,256]{2,1,0:T(8,128)(2,1)} %param.27), channel_id=1, source_target_pairs={{0,1},{1,2},{2,3},{3,0},{4,5},{5,6},{6,7},{7,4},{8,9},{9,10},{10,1... | collective-permute-start | bytes 12582920 | tf_op jit(solution)/shard_map/ppermute | solution.py:23
  134.5 2.6 copy-start.2
  147.2 2.6 copy-start.2
  232.0 146.5 %collective-permute-start.4 = (bf16[4,2048,256]{2,1,0:T(8,128)(2,1)}, bf16[4,2048,256]{2,1,0:T(8,128)(2,1)}, u32[]{:S(2)}, u32[]{:S(2)}) collective-permute-start(bf16[4,2048,256]{2,1,0:T(8,128)(2,1)} %collective-permute-done.3), channel_id=1, source_target_pairs={{0,1},{1,2},{2,3},{3,0},{4,5},{5,6},{6,7},{7,4},{8,9},{9,10},{10,1... | collective-permute-start | bytes 12582920 | tf_op jit(solution)/shard_map/ppermute | solution.py:23
  330.4 18.6 %copy-start.5 = (bf16[4,2048,256]{2,1,0:T(8,128)(2,1)S(1)}, bf16[4,2048,256]{2,1,0:T(8,128)(2,1)}, u32[]{:S(2)}) copy-start(bf16[4,2048,256]{2,1,0:T(8,128)(2,1)} %param.27) | copy-start | bytes 12582916
  349.0 19.0 %copy-start.4 = (bf16[512,4,1024]{2,0,1:T(8,128)(2,1)}, bf16[512,4,1024]{2,0,1:T(8,128)(2,1)S(1)}, u32[]{:S(2)}) copy-start(bf16[512,4,1024]{2,0,1:T(8,128)(2,1)S(1)} %fusion.18) | copy-start | bytes 12582916
  409.3 5.6 copy-start.10
  409.3 5.9 copy-start.12
  409.3 6.1 copy-start.17
  409.3 6.3 copy-start.14
  409.3 8.2 %copy-start.16 = (f32[2048]{0:T(1024)S(1)}, f32[2048]{0:T(1024)}, u32[]{:S(2)}) copy-start(f32[2048]{0:T(1024)} %param.20) | copy-start | bytes 24580
  409.3 189.2 %all-to-all-start.1 = ((bf16[8,64,4,2048]{3,1,2,0:T(8,128)(2,1)}), bf16[8,64,4,2048]{3,1,2,0:T(8,128)(2,1)}, u32[]{:S(2)}, u32[]{:S(2)}) async-start(bf16[8,64,4,2048]{3,1,2,0:T(8,128)(2,1)} %copy.62), calls=%async_computation.2 | async-start | bytes 16777216 | tf_op jit(solution)/shard_map/all_to_all | solution.py:148
  623.1 41.0 %copy-start.1 = (bf16[256,2048]{1,0:T(8,128)(2,1)S(1)}, bf16[256,2048]{1,0:T(8,128)(2,1)}, u32[]{:S(2)}) copy-start(bf16[256,2048]{1,0:T(8,128)(2,1)} %param.19) | copy-start | bytes 3145732
Sparse Core Ops, SparseCore 0:
  9.6 156.1 all-gather.4
  167.3 162.9 all-gather.2
  332.9 71.4 reduce-scatter.1
